TPU v7x, 32 devices: a whole 2x2x4 slice. The times are simulated.
32 devices in a mesh: grp: 2 (over y), sp: 4 (over z), dp: 4 (over x, core).
Axes of the slice: x: 2, y: 2, z: 4, core: 2. Of those that a mesh axis runs over, the one named last changes fastest.
Arguments:
- mixer_source_array: bfloat16 [8, 768, 2048], P(('grp', 'dp'), 'sp'), parts along dimension 0, may hold values from -6 to 6
- source_projection: bfloat16 [2048, 1024], P('dp'), may hold values from -0.125 to 0.125
- gating_projection: bfloat16 [2048, 1024], P('dp'), may hold values from -0.125 to 0.125
- entry_mapping_projection: bfloat16 [2048, 256], replicated, may hold values from -0.0390625 to 0.0390625
- readout_mapping_projection: bfloat16 [2048, 256], replicated, may hold values from -0.0390625 to 0.0390625
- increment_projection: bfloat16 [2048, 16], replicated, may hold values from -0.125 to 0.125
- source_conv_taps: float32 [4, 1024], replicated, may hold values from -3 to 3
- entry_mapping_taps: float32 [4, 256], replicated, may hold values from -3 to 3
- readout_mapping_taps: float32 [4, 256], replicated, may hold values from -3 to 3
- increment_offsets: float32 [16], replicated, may hold values from -1 to 1
- channel_damping_rate: float32 [16], replicated, may hold values from 0 to 1
- bypass_coefficients: float32 [16], replicated, may hold values from 0.5 to 1.5
- stride_multiplier: float32 [8, 768], P(('grp', 'dp')), parts along dimension 0, may hold values from 0.5 to 2
- added_log_damping: float32 [8, 768, 16], P(('grp', 'dp')), parts along dimension 0, may hold values from -2.1 to 0
- norm_scale_factor: float32 [1024], replicated, may hold values from 0.1 to 1.9
- final_projection: bfloat16 [1024, 2048], P(None, 'dp'), may hold values from -0.1875 to 0.1875
Outputs:
- output: bfloat16 [8, 768, 2048], P(('grp', 'dp'), 'sp'), parts along dimension 0
There are 2 independent parts, one for each index of `grp`. A program takes and returns all parts, laid end to end along the dimension named above; an argument that names none is the same for every part. Nothing has to cross between parts.
All inputs are finite; a program needn't handle non-finite values.
Results may differ from a plain program's by a relative error of at most 0.015.
Values may be sent and summed in bfloat16 or wider, within the bound.
A program may use at most 64 MiB of HBM per device.

v0:
```python
import jax
import jax.numpy as jnp
from jax import lax
from jax.sharding import PartitionSpec as P

P_SIZE = 64
N = 128
G = 2
CONV_W = 4
BLK = 64


EPSILON = 1e-06
HIGH = lax.Precision.HIGHEST


def conv_silu(padded, taps):
    width = taps.shape[0]
    length = padded.shape[0] - width + 1
    total = taps[0][None, :] * padded[0:length]
    for shift_pos in range(1, width):
        total = total + taps[shift_pos][None, :] * padded[shift_pos : shift_pos + length]
    return jax.nn.silu(total).astype(jnp.bfloat16)


def block_parts(x_blocks, b_blocks, c_blocks, step_width_value, logarithm_retain):
    cumulative = jnp.cumsum(logarithm_retain, axis=1)
    scaled = (x_blocks.astype(jnp.float32) * step_width_value[..., None]).astype(jnp.bfloat16)
    intersection = jnp.einsum(
        "kign,kjgn->kgij", c_blocks, b_blocks, preferred_element_type=jnp.float32
    )
    by_row = jnp.transpose(cumulative, (0, 2, 3, 1))
    log_gap = by_row[..., :, None] - by_row[..., None, :]
    length = log_gap.shape[-1]
    lower = jnp.tril(jnp.ones((length, length), bool))
    mixing = (intersection[:, :, None] * jnp.exp(jnp.where(lower, log_gap, -jnp.inf))).astype(
        jnp.bfloat16
    )
    inner = jnp.einsum("kgrij,kjgrp->kigrp", mixing, scaled, preferred_element_type=jnp.float32)
    to_end = jnp.exp(cumulative[:, -1:] - cumulative)
    weighted = (b_blocks[:, :, :, None, :].astype(jnp.float32) * to_end[..., None]).astype(
        jnp.bfloat16
    )
    states = jnp.einsum("kjgrn,kjgrp->kgrnp", weighted, scaled, preferred_element_type=jnp.float32)
    return (inner, states, cumulative[:, -1], cumulative)


def block_carry(states, block_total):
    incl_sum = jnp.cumsum(block_total, axis=0)
    excl_sum = incl_sum - block_total
    count = block_total.shape[0]
    log_gap = excl_sum[:, None] - incl_sum[None, :]
    before = (jnp.arange(count)[None, :] < jnp.arange(count)[:, None])[:, :, None, None]
    factors = jnp.exp(jnp.where(before, log_gap, -jnp.inf))
    carried = jnp.einsum("kjgr,jgrnp->kgrnp", factors, states, precision=HIGH)
    final_factor = jnp.exp(incl_sum[-1][None] - incl_sum)
    final_state = jnp.einsum("jgr,jgrnp->grnp", final_factor, states, precision=HIGH)
    return (carried, final_state, excl_sum, incl_sum[-1])


def block_finish(inner, c_blocks, cumulative, carried, x_blocks, skip):
    reached = jnp.einsum("kign,kgrnp->kigrp", c_blocks.astype(jnp.float32), carried, precision=HIGH)
    return (
        inner
        + reached * jnp.exp(cumulative)[..., None]
        + skip[..., None] * x_blocks.astype(jnp.float32)
    )


def heads_mixer(
    proj_x,
    proj_b,
    proj_c,
    step_raw,
    source_conv_taps,
    entry_mapping_taps,
    readout_mapping_taps,
    increment_offsets,
    channel_damping_rate,
    bypass_coefficients,
    tempo_row_values,
    surge_row_values,
):
    tok_rows = proj_x.shape[0]
    head_count = step_raw.shape[1]
    per_group = head_count // G
    shard_head_count = head_count // lax.axis_size("sp")
    leading_head_index = lax.axis_index("sp") * shard_head_count
    b_heads = jnp.broadcast_to(
        proj_b.reshape(tok_rows, G, 1, N), (tok_rows, G, per_group, N)
    ).reshape(tok_rows, head_count, N)
    c_heads = jnp.broadcast_to(
        proj_c.reshape(tok_rows, G, 1, N), (tok_rows, G, per_group, N)
    ).reshape(tok_rows, head_count, N)
    pairs = jnp.stack([b_heads, c_heads], axis=2).reshape(tok_rows, head_count * 2 * N)
    x_arrived, pairs_arrived, step_arrived = (
        lax.all_to_all(proj_x, "sp", split_axis=1, concat_axis=0, tiled=True),
        lax.all_to_all(pairs, "sp", split_axis=1, concat_axis=0, tiled=True),
        lax.all_to_all(step_raw, "sp", split_axis=1, concat_axis=0, tiled=True),
    )
    length = x_arrived.shape[0]
    head_ids = leading_head_index + jnp.arange(shard_head_count)
    group_pick = ((head_ids // per_group)[:, None] == jnp.arange(G)[None, :]).astype(jnp.float32)
    taps_x = lax.dynamic_slice_in_dim(
        source_conv_taps, leading_head_index * P_SIZE, shard_head_count * P_SIZE, 1
    )
    taps_b = jnp.einsum(
        "hg,wgn->whn", group_pick, entry_mapping_taps.reshape(CONV_W, G, N), precision=HIGH
    ).reshape(CONV_W, shard_head_count * N)
    taps_c = jnp.einsum(
        "hg,wgn->whn", group_pick, readout_mapping_taps.reshape(CONV_W, G, N), precision=HIGH
    ).reshape(CONV_W, shard_head_count * N)
    pair_parts = pairs_arrived.reshape(length, shard_head_count, 2, N)
    xs = conv_silu(
        jnp.concatenate(
            [
                jnp.zeros((CONV_W - 1, shard_head_count * P_SIZE), jnp.float32),
                x_arrived.astype(jnp.float32),
            ],
            0,
        ),
        taps_x,
    )
    b_rows = pair_parts[:, :, 0, :].reshape(length, shard_head_count * N).astype(jnp.float32)
    c_rows = pair_parts[:, :, 1, :].reshape(length, shard_head_count * N).astype(jnp.float32)
    bm = conv_silu(
        jnp.concatenate([jnp.zeros((CONV_W - 1, shard_head_count * N), jnp.float32), b_rows], 0),
        taps_b,
    )
    cm = conv_silu(
        jnp.concatenate([jnp.zeros((CONV_W - 1, shard_head_count * N), jnp.float32), c_rows], 0),
        taps_c,
    )
    bias_heads = lax.dynamic_slice_in_dim(
        increment_offsets, leading_head_index, shard_head_count, 0
    )
    speed_per_head = lax.dynamic_slice_in_dim(
        channel_damping_rate, leading_head_index, shard_head_count, 0
    )
    skip_heads = lax.dynamic_slice_in_dim(
        bypass_coefficients, leading_head_index, shard_head_count, 0
    )
    surge_head_values = lax.dynamic_slice_in_dim(
        surge_row_values, leading_head_index, shard_head_count, 1
    )
    step_width_value = jax.nn.softplus(step_arrived.astype(jnp.float32) + bias_heads[None, :])
    logarithm_retain = (
        -speed_per_head[None, :] * step_width_value * tempo_row_values[:, None] + surge_head_values
    )
    blocks = length // BLK
    x_blocks = xs.reshape(blocks, BLK, shard_head_count, 1, P_SIZE)
    b_blocks = bm.reshape(blocks, BLK, shard_head_count, N)
    c_blocks = cm.reshape(blocks, BLK, shard_head_count, N)
    inner, states, block_total, cumulative = block_parts(
        x_blocks,
        b_blocks,
        c_blocks,
        step_width_value.reshape(blocks, BLK, shard_head_count, 1),
        logarithm_retain.reshape(blocks, BLK, shard_head_count, 1),
    )
    carried, final_state, excl_sum, whole_total = block_carry(states, block_total)
    mixed = block_finish(
        inner, c_blocks, cumulative, carried, x_blocks, skip_heads.reshape(shard_head_count, 1)
    )
    mixed = mixed.astype(jnp.bfloat16).reshape(length, shard_head_count * P_SIZE)
    return lax.all_to_all(mixed, "sp", split_axis=0, concat_axis=1, tiled=True)


def shards(
    mixer_source_array,
    source_projection,
    gating_projection,
    entry_mapping_projection,
    readout_mapping_projection,
    increment_projection,
    source_conv_taps,
    entry_mapping_taps,
    readout_mapping_taps,
    increment_offsets,
    channel_damping_rate,
    bypass_coefficients,
    stride_multiplier,
    added_log_damping,
    norm_scale_factor,
    final_projection,
):
    hidden_width = mixer_source_array[0]
    tok_rows = hidden_width.shape[0]
    width_x = source_projection.shape[1]
    acc_x = jnp.dot(
        hidden_width,
        lax.all_gather(source_projection, "dp", axis=0, tiled=True),
        preferred_element_type=jnp.float32,
    )
    acc_z = jnp.dot(
        hidden_width,
        lax.all_gather(gating_projection, "dp", axis=0, tiled=True),
        preferred_element_type=jnp.float32,
    )
    proj_x = acc_x.astype(jnp.bfloat16)
    gate_z = acc_z.astype(jnp.bfloat16)
    proj_b = jnp.dot(
        hidden_width, entry_mapping_projection, preferred_element_type=jnp.float32
    ).astype(jnp.bfloat16)
    proj_c = jnp.dot(
        hidden_width, readout_mapping_projection, preferred_element_type=jnp.float32
    ).astype(jnp.bfloat16)
    step_raw = jnp.dot(
        hidden_width, increment_projection, preferred_element_type=jnp.float32
    ).astype(jnp.bfloat16)
    mixed = heads_mixer(
        proj_x,
        proj_b,
        proj_c,
        step_raw,
        source_conv_taps,
        entry_mapping_taps,
        readout_mapping_taps,
        increment_offsets,
        channel_damping_rate,
        bypass_coefficients,
        stride_multiplier[0],
        added_log_damping[0],
    )
    gated = mixed.astype(jnp.float32) * jax.nn.silu(gate_z.astype(jnp.float32))
    grouped = gated.reshape(tok_rows, G, width_x // G)
    normed = grouped * lax.rsqrt(jnp.mean(grouped * grouped, axis=-1, keepdims=True) + EPSILON)
    normed = (normed.reshape(tok_rows, width_x) * norm_scale_factor[None, :]).astype(jnp.bfloat16)
    output = jnp.dot(
        normed,
        lax.all_gather(final_projection, "dp", axis=1, tiled=True),
        preferred_element_type=jnp.float32,
    ).astype(jnp.bfloat16)
    return output[None]


def solution(mesh):
    return jax.shard_map(
        shards,
        mesh=mesh,
        in_specs=(
            P(("grp", "dp"), "sp", None),
            P("dp", None),
            P("dp", None),
            P(),
            P(),
            P(),
            P(),
            P(),
            P(),
            P(),
            P(),
            P(),
            P(("grp", "dp"), None),
            P(("grp", "dp"), None, None),
            P(),
            P(None, "dp"),
        ),
        out_specs=P(("grp", "dp"), "sp", None),
        check_vma=False,
    )
```

profile of v0, /device:TPU:0, one launch (start us, length us, event | category | flops | bytes accessed | tf_op | source)
XLA Modules:
  0.0 153.6 jit_solution(1723847888486538169)
XLA Ops:
  9.0 6.3 %all-to-all-start.1 = ((bf16[192,4,4]{0,2,1:T(4,128)(2,1)}), bf16[192,4,4]{0,2,1:T(4,128)(2,1)S(1)}, u32[]{:S(2)}, u32[]{:S(2)}) async-start(bf16[192,4,4]{0,2,1:T(4,128)(2,1)} %all_to_all.44), calls=%async_computation.1 | async-start | bytes 16384 | tf_op jit(solution)/shard_map/all_to_all | solution.py:99
  19.6 3.6 %copy.109 = bf16[192,16,2,128]{3,2,1,0:T(2,128)(2,1)} copy(bf16[192,16,2,128]{3,1,0,2:T(8,128)(2,1)S(1)} %pad_maximum_fusion) | data formatting | bytes 3145728 | tf_op jit(solution)/shard_map/stack | solution.py:95
  23.3 2.4 %all_to_all.46 = bf16[192,4,1024]{2,1,0:T(4,128)(2,1)S(1)} reshape(bf16[192,16,2,128]{3,2,1,0:T(2,128)(2,1)} %copy.109) | data formatting | bytes 3145728 | tf_op jit(solution)/shard_map/all_to_all | solution.py:98
  25.6 1.6 %copy.110 = bf16[192,4,1024]{2,0,1:T(8,128)(2,1)} copy(bf16[192,4,1024]{2,1,0:T(4,128)(2,1)S(1)} %all_to_all.46) | data formatting | bytes 3145728 | tf_op jit(solution)/shard_map/all_to_all | solution.py:98
  27.4 5.1 %all-to-all-start.2 = ((bf16[192,4,1024]{2,0,1:T(8,128)(2,1)}), bf16[192,4,1024]{2,0,1:T(8,128)(2,1)}, u32[]{:S(2)}, u32[]{:S(2)}) async-start(bf16[192,4,1024]{2,0,1:T(8,128)(2,1)} %copy.110), calls=%async_computation.2 | async-start | bytes 3145728 | tf_op jit(solution)/shard_map/all_to_all | solution.py:98
  32.9 2.2 %copy.114 = f32[12,64,4,1]{3,0,1,2:T(8,128)} copy(f32[12,64,4,1]{1,0,2,3:T(8,128)S(1)} %fusion.40) | data formatting | bytes 24576 | tf_op jit(solution)/shard_map/add | solution.py:148
  35.0 1.8 %fusion.57 = f32[12,64,4,1]{3,0,1,2:T(8,128)S(1)} fusion(f32[12,64,4,1]{3,0,1,2:T(8,128)} %copy.114), kind=kOutput, calls=%fused_computation.106 | output fusion | flops 193536 | bytes 24576 | tf_op jit(solution)/shard_map/jit(cumsum)/reduce_window_sum | solution.py:27
  38.5 0.9 copy.108
  40.4 28.5 %all-to-all-done.2 = bf16[192,4,1024]{2,0,1:T(8,128)(2,1)} async-done(((bf16[192,4,1024]{2,0,1:T(8,128)(2,1)}), bf16[192,4,1024]{2,0,1:T(8,128)(2,1)}, u32[]{:S(2)}, u32[]{:S(2)}) %all-to-all-start.2) | async-done | bytes 1572896 | tf_op jit(solution)/shard_map/all_to_all | solution.py:98
  69.0 2.8 %reshape.304 = bf16[768,4,2,128]{3,2,1,0:T(2,128)(2,1)S(1)} reshape(bf16[4,192,1024]{2,1,0:T(8,128)(2,1)} %bitcast.14) | data formatting | bytes 3145728 | tf_op jit(solution)/shard_map/reshape | solution.py:113
  71.8 9.9 %fusion.7 = (f32[768,4,128]{2,1,0:T(4,128)}, f32[768,4,128]{2,1,0:T(4,128)S(1)}) fusion(bf16[768,4,2,128]{3,2,1,0:T(2,128)(2,1)S(1)} %reshape.304), kind=kLoop, calls=%fused_computation.10 | loop fusion | flops 786432 | bytes 4718592 | tf_op jit(solution)/shard_map/convert_element_type | solution.py:125
  81.8 1.0 copy-done.3
  82.8 3.2 %convolution_convert_fusion.2 = bf16[192,1024]{1,0:T(8,128)(2,1)S(1)} fusion(bf16[2048,1024]{1,0:T(8,128)(2,1)} %all-gather.4.cloned.1.call-done, bf16[1,192,2048]{2,1,0:T(8,128)(2,1)S(1)} %copy-done.3), kind=kOutput, calls=%fused_computation.29 | convolution fusion | flops 805502976 | bytes 5373952 | tf_op jit(solution)/shard_map/dot_general | solution.py:190
  86.7 4.3 %all-to-all-start = ((bf16[192,4,256]{2,0,1:T(8,128)(2,1)}), bf16[192,4,256]{2,0,1:T(8,128)(2,1)}, u32[]{:S(2)}, u32[]{:S(2)}) async-start(bf16[192,4,256]{2,0,1:T(8,128)(2,1)} %bitcast.130), calls=%async_computation | async-start | bytes 786432 | tf_op jit(solution)/shard_map/all_to_all | solution.py:97
  91.1 1.0 multiply_convert_fusion.2
  92.1 1.1 reshape.307
  94.1 1.0 multiply_convert_fusion.3
  95.1 1.1 reshape.305
  96.2 6.0 %all-to-all-done = bf16[192,4,256]{2,0,1:T(8,128)(2,1)} async-done(((bf16[192,4,256]{2,0,1:T(8,128)(2,1)}), bf16[192,4,256]{2,0,1:T(8,128)(2,1)}, u32[]{:S(2)}, u32[]{:S(2)}) %all-to-all-start) | async-done | bytes 393248 | tf_op jit(solution)/shard_map/all_to_all | solution.py:97
  102.2 1.1 convert_element_type.183
  103.7 1.9 %reshape.310 = f32[12,64,4,64]{3,2,1,0:T(4,128)} reshape(f32[768,256]{1,0:T(8,128)S(1)} %fusion.37) | data formatting | bytes 1572864 | tf_op jit(solution)/shard_map/convert_element_type | solution.py:28
  106.3 2.2 %multiply_convert_fusion.4 = bf16[12,64,4,64]{3,2,1,0:T(4,128)(2,1)S(1)} fusion(f32[12,64,4,64]{3,2,1,0:T(4,128)} %reshape.310, f32[12,64,4]{2,1,0:T(8,128)} %copy.108), kind=kLoop, calls=%fused_computation.26 | loop fusion | flops 393216 | bytes 1191936 | tf_op jit(solution)/shard_map/convert_element_type | solution.py:28
  108.4 1.2 copy.116
  109.6 1.6 %copy.125 = f32[12,64,4,1,64]{1,4,2,0,3:T(8,128)} copy(f32[12,64,4,1,64]{4,2,1,0,3:T(4,128)S(1)} %reshape.315) | data formatting | bytes 1572864 | tf_op jit(solution)/shard_map/convert_element_type | solution.py:28
  111.2 1.7 %fusion.16 = f32[12,4,128,64]{2,3,1,0:T(8,128)S(1)} fusion(bf16[12,64,4,64]{1,3,2,0:T(8,128)(2,1)} %copy.116, f32[12,64,4]{1,2,0:T(4,128)S(1)} %get-tuple-element.10, bf16[12,64,4,128]{3,2,1,0:T(4,128)(2,1)S(1)} %copy-done.5), kind=kOutput, calls=%fused_computation.35 | convolution fusion | flops 51511296 | bytes 2764800 | tf_op jit(solution)/shard_map/kjgrn,kjgrp->kgrnp/dot_general | solution.py:44
  113.0 3.1 %fusion.3 = f32[12,4,128,64]{2,0,3,1:T(8,128)S(1)} fusion(f32[12,4,128,64]{2,3,1,0:T(8,128)S(1)} %fusion.16, f32[12,4]{0,1:T(4,128)S(1)} %bitcast.144, f32[12,4]{0,1:T(4,128)S(1)} %get-tuple-element.7, pred[12,12]{1,0:T(8,128)(4,1)S(1)} %iota_compare_fusion.1), kind=kOutput, calls=%fused_computation.4 | convolution fusion | flops 56624256 | bytes 3146256 | tf_op jit(solution)/shard_map/kjgr,jgrnp->kgrnp/dot_general | solution.py:55
  116.1 2.9 %fusion.11 = f32[12,4,64,64]{3,2,1,0:T(8,128)} fusion(f32[12,4,128,64]{2,0,3,1:T(8,128)S(1)} %fusion.3, bf16[12,64,4,128]{3,2,1,0:T(4,128)(2,1)S(1)} %copy-done.7), kind=kOutput, calls=%fused_computation.16 | convolution fusion | flops 301989888 | bytes 3145728 | tf_op jit(solution)/shard_map/kign,kgrnp->kigrp/dot_general | solution.py:62
  119.0 3.3 %fusion.10 = bf16[12,64,4,1,64]{1,4,2,0,3:T(8,128)(2,1)} fusion(f32[12,4,64,64]{3,2,1,0:T(8,128)} %fusion.11, f32[12,64,4,1,64]{1,4,2,0,3:T(8,128)} %copy.125, bf16[12,64,4,64]{1,3,2,0:T(8,128)(2,1)S(1)} %copy-done.6, f32[4]{0:T(128)S(1)} %dynamic_slice.22, f32[12,64,4]{1,2,0:T(4,128)S(1)} %get-tuple-element.9, f32[12,4,64]{2,1,0:T(4,128)S(1)} %bitcast.142, ...), kind=kOutput, calls=%fused_computation.15 | convolution fusion | flops 77266944 | bytes 3960848 | tf_op jit(solution)/shard_map/kgrij,kjgrp->kigrp/dot_general | solution.py:39
  122.3 1.5 copy.126
  124.3 13.7 %all_to_all.55 = bf16[4,192,256]{2,1,0:T(8,128)(2,1)S(1)} all-to-all(bf16[4,192,256]{2,1,0:T(8,128)(2,1)S(1)} %all_to_all.49), channel_id=1, replica_groups=mesh['grp'=2,'sp'=4,'dp'=4] {'sp'}, dimensions={0} | all-to-all | bytes 786432 | tf_op jit(solution)/shard_map/all_to_all | solution.py:166
  138.1 3.3 %fusion.56 = (f32[192,1024]{1,0:T(8,128)S(1)}, f32[192,1024]{1,0:T(8,128)S(1)}) fusion(f32[192,1024]{1,0:T(8,128)S(1)} %bitcast.139, bf16[2048,1024]{1,0:T(8,128)(2,1)} %all-gather.6.cloned.1.call-done, bf16[1,192,2048]{2,1,0:T(8,128)(2,1)S(1)} %copy-done.3), kind=kOutput, calls=%fused_computation.105 | convolution fusion | flops 806879232 | bytes 7340032 | tf_op jit(solution)/shard_map/dot_general | solution.py:195
  142.9 4.1 %fusion = bf16[1,192,2048]{2,1,0:T(8,128)(2,1)} fusion(bf16[1024,2048]{1,0:T(8,128)(2,1)} %all-gather.8.cloned.1.call-done, f32[192,1024]{1,0:T(8,128)S(1)} %get-tuple-element.24, f32[192,1024]{1,0:T(8,128)S(1)} %bitcast.138, f32[1024]{0:T(1024)S(1)} %copy-done.12), kind=kOutput, calls=%fused_computation.1 | convolution fusion | flops 806289408 | bytes 6557696 | tf_op jit(solution)/shard_map/dot_general | solution.py:229
  (95 shorter events, 14.8 us)
Async XLA Ops:
  6.5 9.6 %copy-start = (bf16[2048,256]{1,0:T(8,128)(2,1)S(1)}, bf16[2048,256]{1,0:T(8,128)(2,1)}, u32[]{:S(2)}) copy-start(bf16[2048,256]{1,0:T(8,128)(2,1)} %param.19) | copy-start | bytes 3145732
  6.5 1.5 copy-start.2
  6.5 1.5 copy-start.9
  6.5 75.3 %all-gather.4.cloned.1.call-start = ((), (), s32[]{:S(2)}) async-start(), calls=%async_computation.4 | async-start | bytes 5242880 | tf_op jit(solution)/shard_map/all_gather | solution.py:192
  7.3 8.8 %copy-start.10 = (f32[4,256]{1,0:T(4,128)S(1)}, f32[4,256]{1,0:T(4,128)}, u32[]{:S(2)}) copy-start(f32[4,256]{1,0:T(4,128)} %param.23) | copy-start | bytes 12292
  7.3 130.9 %all-gather.6.cloned.1.call-start = ((), (), s32[]{:S(2)}) async-start(), calls=%async_computation.5 | async-start | bytes 5242880 | tf_op jit(solution)/shard_map/all_gather | solution.py:197
  9.0 18.4 %all-to-all-start.1 = ((bf16[192,4,4]{0,2,1:T(4,128)(2,1)}), bf16[192,4,4]{0,2,1:T(4,128)(2,1)S(1)}, u32[]{:S(2)}, u32[]{:S(2)}) async-start(bf16[192,4,4]{0,2,1:T(4,128)(2,1)} %all_to_all.44), calls=%async_computation.1 | async-start | bytes 16384 | tf_op jit(solution)/shard_map/all_to_all | solution.py:99
  15.3 1.2 copy-start.8
  15.3 127.5 %all-gather.8.cloned.1.call-start = ((), (), s32[]{:S(2)}) async-start(), calls=%async_computation.6 | async-start | bytes 5242880 | tf_op jit(solution)/shard_map/all_gather | solution.py:231
  18.2 1.1 copy-start.14
  18.2 1.2 copy-start.15
  18.2 1.3 copy-start.13
  25.6 1.6 %copy-start.11 = (f32[4,256]{1,0:T(4,128)S(1)}, f32[4,256]{1,0:T(4,128)}, u32[]{:S(2)}) copy-start(f32[4,256]{1,0:T(4,128)} %param.24) | copy-start | bytes 12292
  25.6 1.7 %copy-start.16 = (f32[16]{0:T(128)S(1)}, f32[16]{0:T(128)}, u32[]{:S(2)}) copy-start(f32[16]{0:T(128)} %param.27) | copy-start | bytes 196
  27.4 41.6 %all-to-all-start.2 = ((bf16[192,4,1024]{2,0,1:T(8,128)(2,1)}), bf16[192,4,1024]{2,0,1:T(8,128)(2,1)}, u32[]{:S(2)}, u32[]{:S(2)}) async-start(bf16[192,4,1024]{2,0,1:T(8,128)(2,1)} %copy.110), calls=%async_computation.2 | async-start | bytes 3145728 | tf_op jit(solution)/shard_map/all_to_all | solution.py:98
  81.7 1.1 copy-start.3
  86.7 15.4 %all-to-all-start = ((bf16[192,4,256]{2,0,1:T(8,128)(2,1)}), bf16[192,4,256]{2,0,1:T(8,128)(2,1)}, u32[]{:S(2)}, u32[]{:S(2)}) async-start(bf16[192,4,256]{2,0,1:T(8,128)(2,1)} %bitcast.130), calls=%async_computation | async-start | bytes 786432 | tf_op jit(solution)/shard_map/all_to_all | solution.py:97
  92.1 1.9 %copy-start.4 = (f32[768,4,128]{2,1,0:T(4,128)S(1)}, f32[768,4,128]{2,1,0:T(4,128)}, u32[]{:S(2)}) copy-start(f32[768,4,128]{2,1,0:T(4,128)} %get-tuple-element.5) | copy-start | bytes 4718596
  109.6 1.6 %copy-start.5 = (bf16[12,64,4,128]{3,2,1,0:T(4,128)(2,1)S(1)}, bf16[12,64,4,128]{3,2,1,0:T(4,128)(2,1)}, u32[]{:S(2)}) copy-start(bf16[12,64,4,128]{3,2,1,0:T(4,128)(2,1)} %reshape.307) | copy-start | bytes 2359300
  113.0 3.1 %copy-start.7 = (bf16[12,64,4,128]{3,2,1,0:T(4,128)(2,1)S(1)}, bf16[12,64,4,128]{3,2,1,0:T(4,128)(2,1)}, u32[]{:S(2)}) copy-start(bf16[12,64,4,128]{3,2,1,0:T(4,128)(2,1)} %reshape.305) | copy-start | bytes 2359300
  116.1 2.9 %copy-start.6 = (bf16[12,64,4,64]{1,3,2,0:T(8,128)(2,1)S(1)}, bf16[12,64,4,64]{1,3,2,0:T(8,128)(2,1)}, u32[]{:S(2)}) copy-start(bf16[12,64,4,64]{1,3,2,0:T(8,128)(2,1)} %copy.116) | copy-start | bytes 1179652
  142.1 0.8 copy-start.12
  142.9 4.2 %copy-start.1 = (bf16[2048,256]{1,0:T(8,128)(2,1)S(1)}, bf16[2048,256]{1,0:T(8,128)(2,1)}, u32[]{:S(2)}) copy-start(bf16[2048,256]{1,0:T(8,128)(2,1)} %param.19) | copy-start | bytes 3145732
Sparse Core Ops, SparseCore 0:
  8.9 37.1 all-gather.3
  47.7 34.4 all-gather.5
  83.7 34.4 all-gather.7
where the time goes:
time: 155 us; the launch traced here: 154 us
  waiting for transfers between devices  36.7 us (24%)
  local copies, waits for them, and re-layouts  32.3 us (21%)
  matrix products  23 us (15%)
  other arithmetic  18.4 us (12%)
  starting transfers between devices  15.8 us (10%)
  blocking collectives  13.7 us (9%)
  between operations  13.6 us (9%)
    all_to_all x1, waiting for transfers between devices, heads_mixer(): lax.all_to_all(pairs, 'sp', split_axis=1, concat_axis=0, tiled=True)  28.5 us
    all_to_all x1, blocking collectives, heads_mixer(): return lax.all_to_all(mixed, 'sp', split_axis=0, concat_axis=1, tiled=True)  13.7 us
    convert_element_type x1, other arithmetic, heads_mixer(): pair_parts[:, :, 1, :].reshape(length, shard_head_count * N)  9.87 us
    all_to_all x1, starting transfers between devices, heads_mixer(): lax.all_to_all(step_raw, 'sp', split_axis=1, concat_axis=0, tiled=True)  6.35 us
    all_to_all x1, waiting for transfers between devices, heads_mixer(): lax.all_to_all(proj_x, 'sp', split_axis=1, concat_axis=0, tiled=True)  6.02 us
    all_to_all x1, starting transfers between devices, heads_mixer(): lax.all_to_all(pairs, 'sp', split_axis=1, concat_axis=0, tiled=True)  5.09 us
    all_to_all x1, starting transfers between devices, heads_mixer(): lax.all_to_all(proj_x, 'sp', split_axis=1, concat_axis=0, tiled=True)  4.35 us
    dot_general x1, matrix products, shards(): jnp.dot(normed, lax.all_gather(final_projection, 'dp', axis=1, tiled=True...  4.15 us
  transfers between devices with their start and end apart: 6, of which 2 were waited for; matrix products, arithmetic and copies ran while one was open for 42% of the time, Pallas kernels for 0%

commit v1 on v0

v1 whole, which is shorter than its diff:
```python
import functools

import jax
import jax.numpy as jnp
from jax import lax
from jax.experimental import pallas as pl
from jax.experimental.pallas import tpu as pltpu
from jax.sharding import PartitionSpec as P

P_SIZE = 64
N = 128
G = 2
CONV_W = 4
EPSILON = 1e-06
HIGH = lax.Precision.HIGHEST
MESH = pl.DeviceIdType.MESH
HALO = 16
F32 = jnp.float32
BF16 = jnp.bfloat16


def dot(a, b, dims=((1,), (0,)), precision=None):
    return lax.dot_general(a, b, (dims, ((), ())), precision=precision, preferred_element_type=F32)


def silu(v):
    return v * (1.0 / (1.0 + jnp.exp(-v)))


def kernel(
    dims,
    x_hbm,
    wx_hbm,
    wz_hbm,
    wf_hbm,
    wb_ref,
    wc_ref,
    wdt_ref,
    tx_ref,
    tb_ref,
    tc_ref,
    off_ref,
    rate_ref,
    skip_ref,
    stride_ref,
    damp_ref,
    scale_ref,
    out_ref,
    xe,
    wx,
    wz,
    wf,
    pbc,
    px,
    bm,
    cm,
    xs,
    sc,
    y,
    st,
    car,
    snd,
    nrm,
    loc_sem,
    halo_send,
    halo_recv,
    x_send,
    x_recv,
    y_send,
    y_recv,
    d_send,
    d_recv,
    c_send,
    c_recv,
):
    n_grp, n_sp, n_dp, chunks, c_chunks = dims
    n_x = n_dp // 2
    grp, z, dp = (lax.axis_index(a) for a in ("grp", "sp", "dp"))
    xi, core = dp // 2, dp % 2
    tok = out_ref.shape[0]
    width = xs.shape[1]
    heads = off_ref.shape[1]
    per_group = heads // G
    gw = width // G
    partner = {"dp": xi * 2 + 1 - core}
    y_peer = {"grp": 1 - grp}
    srcs = (wx_hbm, wz_hbm, wf_hbm)

    def at(w, owner, start, rows):
        if w == 2:
            return wf.at[owner, pl.ds(start, rows)]
        ref = (wx, wz)[w]
        return ref.at[pl.ds(pl.multiple_of(owner * srcs[w].shape[0] + start, 16), rows)]

    barrier = pltpu.get_barrier_semaphore()
    peers = [partner, y_peer]
    peers += [{"dp": lax.rem(xi + o, n_x) * 2 + core} for o in range(1, n_x)]
    for peer in peers:
        pl.semaphore_signal(barrier, inc=1, device_id=peer, device_id_type=MESH)

    @pl.when(z > 0)
    def _():
        pl.semaphore_signal(barrier, inc=1, device_id={"sp": z - 1}, device_id_type=MESH)

    @pl.when(z < n_sp - 1)
    def _():
        pl.semaphore_signal(barrier, inc=1, device_id={"sp": z + 1}, device_id_type=MESH)

    x_copy = pltpu.make_async_copy(x_hbm, xe.at[pl.ds(HALO, tok)], loc_sem.at[3])
    x_copy.start()
    own = []
    for w in range(3):
        copy = pltpu.make_async_copy(srcs[w], at(w, dp, 0, srcs[w].shape[0]), loc_sem.at[w])
        copy.start()
        own.append(copy)

    pl.semaphore_wait(barrier, len(peers) + jnp.minimum(z, 1) + jnp.minimum(n_sp - 1 - z, 1))

    def remote(src, dst, send, recv, peer):
        return pltpu.make_async_remote_copy(
            src_ref=src, dst_ref=dst, send_sem=send, recv_sem=recv,
            device_id=peer, device_id_type=MESH,
        )

    def halo_copy():
        return remote(
            x_hbm.at[pl.ds(tok - HALO, HALO)], xe.at[pl.ds(0, HALO)],
            halo_send, halo_recv, {"sp": jnp.minimum(z + 1, n_sp - 1)},
        )

    @pl.when(z < n_sp - 1)
    def _():
        halo_copy().start()

    sends = []

    def x_copy_of(w, o, k, owner, src=None):
        half = srcs[w].shape[0] // n_grp
        rows = half // chunks
        start = grp * half + k * rows
        place = at(w, owner, start, rows)
        if src is not None:
            src = src.at[pl.ds(start, rows)]
        return remote(
            place if src is None else src, place,
            x_send.at[w, o - 1, k], x_recv.at[w, o - 1, k],
            {"dp": lax.rem(xi + o, n_x) * 2 + core},
        )

    for w in range(3):
        for k in range(chunks):
            for o in range(1, n_x):
                copy = x_copy_of(w, o, k, dp, srcs[w])
                copy.start()
                sends.append(copy)
        copy = remote(
            srcs[w], at(w, dp, 0, srcs[w].shape[0]), d_send.at[w, 0], d_recv.at[w], partner
        )
        copy.start()
        sends.append(copy)

    def owner_of(o):
        return lax.rem(xi - o + n_x, n_x) * 2 + core

    def pump(w, k):
        half = srcs[w].shape[0] // n_grp
        rows = half // chunks
        for o in range(1, n_x):
            x_copy_of(w, o, k, owner_of(o)).wait_recv()
            place = at(w, owner_of(o), grp * half + k * rows, rows)
            copy = remote(place, place, y_send.at[w, o - 1, k], y_recv.at[w, o - 1], y_peer)
            copy.start()
            sends.append(copy)
            if k == chunks - 1:
                place = at(w, owner_of(o), grp * half, half)
                copy = remote(place, place, d_send.at[w, o], d_recv.at[w], partner)
                copy.start()
                sends.append(copy)

    def finish(w):
        half = srcs[w].shape[0] // n_grp
        for o in range(1, n_x):
            place = at(w, owner_of(o), (1 - grp) * half, half)
            remote(place, place, y_send.at[w, o - 1, 0], y_recv.at[w, o - 1], y_peer).wait_recv()
            copy = remote(place, place, d_send.at[w, n_x - 1 + o], d_recv.at[w], partner)
            copy.start()
            sends.append(copy)
        own[w].wait()
        if w == 2:
            place = wf.at[pl.ds(0, n_x)]
        else:
            place = (wx, wz)[w].at[pl.ds(0, n_x * srcs[w].shape[0])]
        remote(place, place, d_send.at[w, 0], d_recv.at[w], partner).wait_recv()

    @pl.when(z == 0)
    def _():
        xe[pl.ds(0, HALO), :] = jnp.zeros((HALO, xe.shape[1]), BF16)

    @pl.when(z > 0)
    def _():
        halo_copy().wait_recv()

    x_copy.wait()
    gn = G * N
    pbc[:, 0:gn] = dot(xe[...], wb_ref[...]).astype(BF16).astype(F32)
    pbc[:, gn : 2 * gn] = dot(xe[...], wc_ref[...]).astype(BF16).astype(F32)
    raw = dot(xe[pl.ds(HALO, tok), :], wdt_ref[...]).astype(BF16).astype(F32)

    def conv(buf, cols, taps):
        total = taps[0:1, :] * buf[pl.ds(HALO - CONV_W + 1, tok), cols]
        for k in range(1, CONV_W):
            total = total + taps[k : k + 1, :] * buf[pl.ds(HALO - CONV_W + 1 + k, tok), cols]
        return silu(total).astype(BF16)

    bm[...] = conv(pbc, pl.ds(0, gn), tb_ref[...])
    cm[...] = conv(pbc, pl.ds(gn, gn), tc_ref[...])
    pre = raw + off_ref[...]
    step = jnp.maximum(pre, 0.0) + jnp.log1p(jnp.exp(-jnp.abs(pre)))
    length = stride_ref.shape[1]
    here = lax.broadcasted_iota(jnp.int32, (tok, length), 0) + z * tok
    at_pos = here == lax.broadcasted_iota(jnp.int32, (tok, length), 1)
    tempo = jnp.sum(jnp.where(at_pos, stride_ref[...], 0.0), axis=1, keepdims=True)
    damp = damp_ref[0, pl.ds(pl.multiple_of(z * tok, 8), tok), :]
    keep = -rate_ref[...] * step * tempo + damp
    row = lax.broadcasted_iota(jnp.int32, (tok, tok), 0)
    col = lax.broadcasted_iota(jnp.int32, (tok, tok), 1)
    lower = row >= col
    cum = dot(lower.astype(F32), keep, precision=HIGH)
    cum_t = dot(keep, (row <= col).astype(F32), ((0,), (0,)), HIGH)
    last = cum[tok - 1 : tok, :]
    to_end = jnp.exp(last - cum)
    reach = jnp.exp(cum)
    whole = jnp.exp(last)
    first_head = lax.broadcasted_iota(jnp.int32, (tok, 2 * P_SIZE), 1) < P_SIZE
    first_row = first_head[0:1, :]

    def spread(values, p, mask):
        return jnp.where(mask, values[:, 2 * p : 2 * p + 1], values[:, 2 * p + 1 : 2 * p + 2])

    def pair_cols(p):
        return pl.ds(p * 2 * P_SIZE, 2 * P_SIZE)

    for k in range(chunks):
        pump(0, k)
    finish(0)

    tile = 256

    def project_x(j, carry):
        cols = pl.ds(pl.multiple_of(j * tile, tile), tile)
        px[:, cols] = dot(xe[...], wx[:, cols]).astype(BF16).astype(F32)
        xs[:, cols] = conv(px, cols, tx_ref[:, cols])
        return carry

    lax.fori_loop(0, width // tile, project_x, 0)
    pump(1, 0)

    scaled = []
    for p in range(heads // 2):
        xp = xs[:, pair_cols(p)].astype(F32)
        s = (xp * spread(step, p, first_head)).astype(BF16)
        sc[:, pair_cols(p)] = (s.astype(F32) * spread(to_end, p, first_head)).astype(BF16)
        y[:, pair_cols(p)] = spread(skip_ref[...], p, first_row) * xp
        scaled.append(s)
    for g in range(G):
        cols = pl.ds(g * gw, gw)
        st[:, cols] = dot(bm[:, g * N : (g + 1) * N], sc[:, cols], ((0,), (0,)))

    cw = width // c_chunks

    def chain_copy(j):
        cols = pl.ds(j * cw, cw)
        return remote(
            snd.at[:, cols], car.at[:, cols], c_send.at[j], c_recv.at[j],
            {"sp": jnp.minimum(z + 1, n_sp - 1)},
        )

    def chain(j):
        cols = pl.ds(j * cw, cw)

        @pl.when(z == 0)
        def _():
            car[:, cols] = jnp.zeros((N, cw), BF16)

        @pl.when(z > 0)
        def _():
            chain_copy(j).wait_recv()

        @pl.when(z < n_sp - 1)
        def _():
            for p in range(j * cw // (2 * P_SIZE), (j + 1) * cw // (2 * P_SIZE)):
                pc = pair_cols(p)
                total = spread(whole, p, first_row) * car[:, pc].astype(F32) + st[:, pc]
                snd[:, pc] = total.astype(BF16)
            chain_copy(j).start()

    def inner(g):
        cb = dot(cm[:, g * N : (g + 1) * N], bm[:, g * N : (g + 1) * N], ((1,), (1,)))
        for p in range(g * per_group // 2, (g + 1) * per_group // 2):
            parts = []
            for h in (2 * p, 2 * p + 1):
                gap = jnp.where(lower, cum[:, h : h + 1] - cum_t[h : h + 1, :], -jnp.inf)
                parts.append(dot((cb * jnp.exp(gap)).astype(BF16), scaled[p]))
            y[:, pair_cols(p)] += jnp.where(first_head, parts[0], parts[1])

    for k in range(1, chunks):
        pump(1, k)
    for g in range(G):
        inner(g)
    for k in range(max(chunks, c_chunks)):
        if k < c_chunks:
            chain(k)
        if k < chunks:
            pump(2, k)
    finish(1)

    for g in range(G):
        cols = pl.ds(g * gw, gw)
        reached = dot(cm[:, g * N : (g + 1) * N], car[:, cols])
        gate = silu(dot(xe[pl.ds(HALO, tok), :], wz[:, cols]).astype(BF16).astype(F32))
        square = jnp.zeros((tok, 1), F32)
        first = g * per_group // 2
        for p in range(first, first + per_group // 2):
            here = slice((p - first) * 2 * P_SIZE, (p - first + 1) * 2 * P_SIZE)
            mixed = y[:, pair_cols(p)] + spread(reach, p, first_head) * reached[:, here]
            gated = mixed.astype(BF16).astype(F32) * gate[:, here]
            square = square + jnp.sum(gated * gated, axis=1, keepdims=True)
            y[:, pair_cols(p)] = gated
        inv = lax.rsqrt(square * (1.0 / gw) + EPSILON)
        nrm[:, cols] = (y[:, cols] * inv * scale_ref[:, cols]).astype(BF16)

    finish(2)
    fw = wf.shape[2]
    for d in range(n_dp):
        out_ref[:, d * fw : (d + 1) * fw] = dot(nrm[...], wf[d]).astype(BF16)

    for copy in sends:
        copy.wait_send()

    @pl.when(z < n_sp - 1)
    def _():
        halo_copy().wait_send()
        for j in range(c_chunks):
            chain_copy(j).wait_send()


def shards(
    dims,
    mixer_source_array,
    source_projection,
    gating_projection,
    entry_mapping_projection,
    readout_mapping_projection,
    increment_projection,
    source_conv_taps,
    entry_mapping_taps,
    readout_mapping_taps,
    increment_offsets,
    channel_damping_rate,
    bypass_coefficients,
    stride_multiplier,
    added_log_damping,
    norm_scale_factor,
    final_projection,
):
    n_grp, n_sp, n_dp, chunks, c_chunks = dims
    n_x = n_dp // 2
    hidden = mixer_source_array[0]
    tok, model = hidden.shape
    width = source_projection.shape[1]
    gn = G * N
    out_width = final_projection.shape[1] * n_dp
    dma = pltpu.SemaphoreType.DMA
    remote_srcs = max(n_x - 1, 1)
    vmem = pl.BlockSpec(memory_space=pltpu.VMEM)
    hbm = pl.BlockSpec(memory_space=pl.ANY)
    output = pl.pallas_call(
        functools.partial(kernel, dims),
        out_shape=jax.ShapeDtypeStruct((tok, out_width), BF16),
        in_specs=[hbm] * 4 + [vmem] * 12,
        out_specs=vmem,
        scratch_shapes=[
            pltpu.VMEM((HALO + tok, model), BF16),
            pltpu.VMEM((model, width), BF16),
            pltpu.VMEM((model, width), BF16),
            pltpu.VMEM((n_dp,) + final_projection.shape, BF16),
            pltpu.VMEM((HALO + tok, 2 * gn), F32),
            pltpu.VMEM((HALO + tok, width), F32),
            pltpu.VMEM((tok, gn), BF16),
            pltpu.VMEM((tok, gn), BF16),
            pltpu.VMEM((tok, width), BF16),
            pltpu.VMEM((tok, width), BF16),
            pltpu.VMEM((tok, width), F32),
            pltpu.VMEM((N, width), F32),
            pltpu.VMEM((N, width), BF16),
            pltpu.VMEM((N, width), BF16),
            pltpu.VMEM((tok, width), BF16),
            dma((4,)),
            dma,
            dma,
            dma((3, remote_srcs, chunks)),
            dma((3, remote_srcs, chunks)),
            dma((3, remote_srcs, chunks)),
            dma((3, remote_srcs)),
            dma((3, 2 * n_x - 1)),
            dma((3,)),
            dma((c_chunks,)),
            dma((c_chunks,)),
        ],
        compiler_params=pltpu.CompilerParams(
            collective_id=0, has_side_effects=True, vmem_limit_bytes=56 * 1024 * 1024
        ),
    )(
        hidden,
        source_projection,
        gating_projection,
        final_projection,
        entry_mapping_projection,
        readout_mapping_projection,
        increment_projection,
        source_conv_taps,
        entry_mapping_taps,
        readout_mapping_taps,
        increment_offsets[None],
        channel_damping_rate[None],
        bypass_coefficients[None],
        stride_multiplier,
        added_log_damping,
        norm_scale_factor[None],
    )
    return output[None]


def solution(mesh):
    n_grp, n_sp, n_dp = (mesh.shape[a] for a in ("grp", "sp", "dp"))
    chunks = 4 if n_dp <= 4 else 1
    return jax.shard_map(
        functools.partial(shards, (n_grp, n_sp, n_dp, chunks, 4)),
        mesh=mesh,
        in_specs=(
            P(("grp", "dp"), "sp", None),
            P("dp", None),
            P("dp", None),
            P(),
            P(),
            P(),
            P(),
            P(),
            P(),
            P(),
            P(),
            P(),
            P(("grp", "dp"), None),
            P(("grp", "dp"), None, None),
            P(),
            P(None, "dp"),
        ),
        out_specs=P(("grp", "dp"), "sp", None),
        check_vma=False,
    )
```

time: 155 us -> 60.1 us (0.39)
  the two profiles are of different devices: /device:TPU:0 before, /device:TPU:25 now
where the time goes in v1:
time: 60.1 us; the launch traced here: 59.8 us
  Pallas kernels  55 us (92%)
  local copies, waits for them, and re-layouts  4.84 us (8%)
    pallas_call x1, Pallas kernels, shards(): pl.pallas_call(functools.partial(kernel, dims), out_shape=jax.ShapeDtypeS...  55 us
    unnamed x5, local copies, waits for them, and re-layouts  4.84 us

profile of v1, /device:TPU:25, one launch (start us, length us, event | category | flops | bytes accessed | tf_op | source)
XLA Modules:
  0.0 59.8 jit_solution(4863691868115669302)
XLA Ops:
  0.0 0.0 copy-start
  0.0 1.7 %copy.18.damp_ref = f32[1,768,16]{2,1,0:T(8,128)} copy(f32[1,768,16]{1,2,0:T(8,128)} %param.29) | data formatting | bytes 98304 | tf_op args[13]
  1.7 0.0 copy-done
  1.7 1.0 %copy.17.wdt_ref = bf16[2048,16]{1,0:T(8,128)(2,1)} copy(bf16[2048,16]{0,1:T(8,128)(2,1)S(1)} %copy-done) | data formatting | bytes 131072 | tf_op args[5]
  2.7 55.0 %shard_map.154 = bf16[192,2048]{1,0:T(8,128)(2,1)} custom-call(bf16[192,2048]{1,0:T(8,128)(2,1)} %bitcast.7, bf16[512,1024]{1,0:T(8,128)(2,1)} %wx_hbm.1, bf16[512,1024]{1,0:T(8,128)(2,1)} %wz_hbm.1, bf16[1024,512]{1,0:T(8,128)(2,1)} %wf_hbm.1, bf16[2048,256]{1,0:T(8,128)(2,1)} %wb_ref.1, bf16[2048,256]{1,0:T(8,128)(2,1)} %wc_ref.1, ...), custom_call_target="tpu_custom_call" | custom-call | tf_op jit(solution)/shard_map/pallas_call | solution.py:377
  57.8 2.1 %copy.20 = bf16[1,192,2048]{2,1,0:T(8,128)(2,1)} copy(bf16[1,192,2048]{2,1,0:T(8,128)(2,1)} %bitcast.6) | data formatting | bytes 1572864
Async XLA Ops:
  0.0 1.7 %copy-start = (bf16[2048,16]{0,1:T(8,128)(2,1)S(1)}, bf16[2048,16]{0,1:T(8,128)(2,1)}, u32[]{:S(2)}) copy-start(bf16[2048,16]{0,1:T(8,128)(2,1)} %param.21) | copy-start | bytes 196612

commit v2 on v1

--- a/solution.py
+++ b/solution.py
@@ -33,9 +33,9 @@
     wx_hbm,
     wz_hbm,
     wf_hbm,
-    wb_ref,
-    wc_ref,
-    wdt_ref,
+    wb_hbm,
+    wc_hbm,
+    wdt_hbm,
     tx_ref,
     tb_ref,
     tc_ref,
@@ -45,7 +45,7 @@
     stride_ref,
     damp_ref,
     scale_ref,
-    out_ref,
+    out_hbm,
     xe,
     wx,
     wz,
@@ -61,6 +61,9 @@
     car,
     snd,
     nrm,
+    out_ref,
+    wbc,
+    wdt,
     loc_sem,
     halo_send,
     halo_recv,
@@ -68,12 +71,15 @@
     x_recv,
     y_send,
     y_recv,
+    z_send,
+    z_recv,
     d_send,
     d_recv,
     c_send,
     c_recv,
+    o_sem,
 ):
-    n_grp, n_sp, n_dp, chunks, c_chunks = dims
+    n_grp, n_sp, n_dp, c_chunks = dims
     n_x = n_dp // 2
     grp, z, dp = (lax.axis_index(a) for a in ("grp", "sp", "dp"))
     xi, core = dp // 2, dp % 2
@@ -84,6 +90,8 @@
     gw = width // G
     partner = {"dp": xi * 2 + 1 - core}
     y_peer = {"grp": 1 - grp}
+    zb = z % 2
+    z_peer = {"sp": z + 1 - 2 * zb}
     srcs = (wx_hbm, wz_hbm, wf_hbm)
 
     def at(w, owner, start, rows):
@@ -106,8 +114,16 @@
     def _():
         pl.semaphore_signal(barrier, inc=1, device_id={"sp": z + 1}, device_id_type=MESH)
 
+    gn = G * N
     x_copy = pltpu.make_async_copy(x_hbm, xe.at[pl.ds(HALO, tok)], loc_sem.at[3])
     x_copy.start()
+    maps = [
+        pltpu.make_async_copy(wb_hbm, wbc.at[:, pl.ds(0, gn)], loc_sem.at[4]),
+        pltpu.make_async_copy(wc_hbm, wbc.at[:, pl.ds(gn, gn)], loc_sem.at[5]),
+        pltpu.make_async_copy(wdt_hbm, wdt, loc_sem.at[6]),
+    ]
+    for copy in maps:
+        copy.start()
     own = []
     for w in range(3):
         copy = pltpu.make_async_copy(srcs[w], at(w, dp, 0, srcs[w].shape[0]), loc_sem.at[w])
@@ -134,63 +150,81 @@
 
     sends = []
 
-    def x_copy_of(w, o, k, owner, src=None):
-        half = srcs[w].shape[0] // n_grp
-        rows = half // chunks
-        start = grp * half + k * rows
+    def half_of(w):
+        return srcs[w].shape[0] // 8
+
+    def owner_of(o):
+        return lax.rem(xi - o + n_x, n_x) * 2 + core
+
+    own_q = grp * 2 + zb
+    y_q = (1 - grp) * 2 + zb
+    z_q = grp * 2 + 1 - zb
+    far_q = (1 - grp) * 2 + 1 - zb
+
+    def x_piece(w, o, k, owner, src=None):
+        rows = half_of(w)
+        start = far_q * 2 * rows + rows if k == 2 else own_q * 2 * rows + k * rows
         place = at(w, owner, start, rows)
         if src is not None:
-            src = src.at[pl.ds(start, rows)]
+            src = src.at[pl.ds(pl.multiple_of(start, 16), rows)]
         return remote(
             place if src is None else src, place,
             x_send.at[w, o - 1, k], x_recv.at[w, o - 1, k],
             {"dp": lax.rem(xi + o, n_x) * 2 + core},
         )
 
-    for w in range(3):
-        for k in range(chunks):
-            for o in range(1, n_x):
-                copy = x_copy_of(w, o, k, dp, srcs[w])
-                copy.start()
-                sends.append(copy)
-        copy = remote(
-            srcs[w], at(w, dp, 0, srcs[w].shape[0]), d_send.at[w, 0], d_recv.at[w], partner
-        )
+    def y_piece(w, o, k, quarter, part):
+        place = at(w, owner_of(o), (quarter * 2 + part) * half_of(w), half_of(w))
+        return remote(place, place, y_send.at[w, o - 1, k], y_recv.at[w, o - 1, k], y_peer)
+
+    def z_piece(w, o, k, quarter):
+        place = at(w, owner_of(o), (quarter * 2 + k) * half_of(w), half_of(w))
+        return remote(place, place, z_send.at[w, o - 1, k], z_recv.at[w, o - 1, k], z_peer)
+
+    def d_piece(w, o, k, quarter):
+        place = at(w, owner_of(o), quarter * 2 * half_of(w), 2 * half_of(w))
+        return remote(place, place, d_send.at[w, o, k], d_recv.at[w], partner)
+
+    def start(copy):
         copy.start()
         sends.append(copy)
 
-    def owner_of(o):
-        return lax.rem(xi - o + n_x, n_x) * 2 + core
+    for w in range(3):
+        for k in range(3):
+            for o in range(1, n_x):
+                start(x_piece(w, o, k, dp, srcs[w]))
+        rows = srcs[w].shape[0]
+        start(remote(srcs[w], at(w, dp, 0, rows), d_send.at[w, 0, 0], d_recv.at[w], partner))
 
     def pump(w, k):
-        half = srcs[w].shape[0] // n_grp
-        rows = half // chunks
         for o in range(1, n_x):
-            x_copy_of(w, o, k, owner_of(o)).wait_recv()
-            place = at(w, owner_of(o), grp * half + k * rows, rows)
-            copy = remote(place, place, y_send.at[w, o - 1, k], y_recv.at[w, o - 1], y_peer)
-            copy.start()
-            sends.append(copy)
-            if k == chunks - 1:
-                place = at(w, owner_of(o), grp * half, half)
-                copy = remote(place, place, d_send.at[w, o], d_recv.at[w], partner)
-                copy.start()
-                sends.append(copy)
+            if k < 2:
+                x_piece(w, o, k, owner_of(o)).wait_recv()
+                start(y_piece(w, o, k, own_q, k))
+                start(z_piece(w, o, k, own_q))
+                if k == 1:
+                    start(d_piece(w, o, 0, own_q))
+            elif k == 2:
+                z_piece(w, o, 0, z_q).wait_recv()
+                start(y_piece(w, o, 2, z_q, 0))
+            elif k == 3:
+                z_piece(w, o, 1, z_q).wait_recv()
+                start(d_piece(w, o, 1, z_q))
+                y_piece(w, o, 0, y_q, 0).wait_recv()
+                y_piece(w, o, 1, y_q, 1).wait_recv()
+                start(d_piece(w, o, 2, y_q))
+            else:
+                y_piece(w, o, 2, far_q, 0).wait_recv()
+                x_piece(w, o, 2, owner_of(o)).wait_recv()
+                start(d_piece(w, o, 3, far_q))
 
     def finish(w):
-        half = srcs[w].shape[0] // n_grp
-        for o in range(1, n_x):
-            place = at(w, owner_of(o), (1 - grp) * half, half)
-            remote(place, place, y_send.at[w, o - 1, 0], y_recv.at[w, o - 1], y_peer).wait_recv()
-            copy = remote(place, place, d_send.at[w, n_x - 1 + o], d_recv.at[w], partner)
-            copy.start()
-            sends.append(copy)
         own[w].wait()
         if w == 2:
             place = wf.at[pl.ds(0, n_x)]
         else:
             place = (wx, wz)[w].at[pl.ds(0, n_x * srcs[w].shape[0])]
-        remote(place, place, d_send.at[w, 0], d_recv.at[w], partner).wait_recv()
+        remote(place, place, d_send.at[w, 0, 0], d_recv.at[w], partner).wait_recv()
 
     @pl.when(z == 0)
     def _():
@@ -201,10 +235,10 @@
         halo_copy().wait_recv()
 
     x_copy.wait()
-    gn = G * N
-    pbc[:, 0:gn] = dot(xe[...], wb_ref[...]).astype(BF16).astype(F32)
-    pbc[:, gn : 2 * gn] = dot(xe[...], wc_ref[...]).astype(BF16).astype(F32)
-    raw = dot(xe[pl.ds(HALO, tok), :], wdt_ref[...]).astype(BF16).astype(F32)
+    for copy in maps:
+        copy.wait()
+    pbc[...] = dot(xe[...], wbc[...]).astype(BF16).astype(F32)
+    raw = dot(wdt[...], xe[pl.ds(HALO, tok), :], ((1,), (1,))).astype(BF16).astype(F32)
 
     def conv(buf, cols, taps):
         total = taps[0:1, :] * buf[pl.ds(HALO - CONV_W + 1, tok), cols]
@@ -214,19 +248,29 @@
 
     bm[...] = conv(pbc, pl.ds(0, gn), tb_ref[...])
     cm[...] = conv(pbc, pl.ds(gn, gn), tc_ref[...])
-    pre = raw + off_ref[...]
-    step = jnp.maximum(pre, 0.0) + jnp.log1p(jnp.exp(-jnp.abs(pre)))
-    length = stride_ref.shape[1]
-    here = lax.broadcasted_iota(jnp.int32, (tok, length), 0) + z * tok
-    at_pos = here == lax.broadcasted_iota(jnp.int32, (tok, length), 1)
-    tempo = jnp.sum(jnp.where(at_pos, stride_ref[...], 0.0), axis=1, keepdims=True)
-    damp = damp_ref[0, pl.ds(pl.multiple_of(z * tok, 8), tok), :]
-    keep = -rate_ref[...] * step * tempo + damp
-    row = lax.broadcasted_iota(jnp.int32, (tok, tok), 0)
-    col = lax.broadcasted_iota(jnp.int32, (tok, tok), 1)
+
+    def square_iota(size):
+        return [lax.broadcasted_iota(jnp.int32, (size, size), d) for d in (0, 1)]
+
+    def column(ref):
+        i, j = square_iota(heads)
+        return jnp.sum(jnp.where(i == j, ref[...], 0.0), axis=1, keepdims=True)
+
+    def my_positions(values):
+        mine = values[:, 0:tok]
+        for i in range(1, n_sp):
+            mine = jnp.where(z == i, values[:, i * tok : (i + 1) * tok], mine)
+        return mine
+
+    pre = raw + column(off_ref)
+    step_t = jnp.maximum(pre, 0.0) + jnp.log1p(jnp.exp(-jnp.abs(pre)))
+    tempo = my_positions(stride_ref[...])
+    keep = -column(rate_ref) * step_t * tempo + my_positions(damp_ref[0])
+    row, col = square_iota(tok)
     lower = row >= col
-    cum = dot(lower.astype(F32), keep, precision=HIGH)
-    cum_t = dot(keep, (row <= col).astype(F32), ((0,), (0,)), HIGH)
+    step = dot((row == col).astype(F32), step_t, ((1,), (1,)), HIGH)
+    cum = dot(lower.astype(F32), keep, ((1,), (1,)), HIGH)
+    cum_t = dot(keep, (row <= col).astype(F32), precision=HIGH)
     last = cum[tok - 1 : tok, :]
     to_end = jnp.exp(last - cum)
     reach = jnp.exp(cum)
@@ -240,9 +284,12 @@
     def pair_cols(p):
         return pl.ds(p * 2 * P_SIZE, 2 * P_SIZE)
 
-    for k in range(chunks):
+    for k in range(4):
         pump(0, k)
+    pump(1, 0)
+    pump(0, 4)
     finish(0)
+    pump(1, 1)
 
     tile = 256
 
@@ -253,7 +300,8 @@
         return carry
 
     lax.fori_loop(0, width // tile, project_x, 0)
-    pump(1, 0)
+    pump(1, 2)
+    pump(1, 3)
 
     scaled = []
     for p in range(heads // 2):
@@ -275,24 +323,27 @@
             {"sp": jnp.minimum(z + 1, n_sp - 1)},
         )
 
-    def chain(j):
+    def chain_first(j):
         cols = pl.ds(j * cw, cw)
 
         @pl.when(z == 0)
         def _():
             car[:, cols] = jnp.zeros((N, cw), BF16)
-
+            snd[:, cols] = st[:, cols].astype(BF16)
+            chain_copy(j).start()
+
+    def chain(j):
         @pl.when(z > 0)
         def _():
             chain_copy(j).wait_recv()
 
-        @pl.when(z < n_sp - 1)
-        def _():
-            for p in range(j * cw // (2 * P_SIZE), (j + 1) * cw // (2 * P_SIZE)):
-                pc = pair_cols(p)
-                total = spread(whole, p, first_row) * car[:, pc].astype(F32) + st[:, pc]
-                snd[:, pc] = total.astype(BF16)
-            chain_copy(j).start()
+            @pl.when(z < n_sp - 1)
+            def _():
+                for p in range(j * cw // (2 * P_SIZE), (j + 1) * cw // (2 * P_SIZE)):
+                    pc = pair_cols(p)
+                    total = spread(whole, p, first_row) * car[:, pc].astype(F32) + st[:, pc]
+                    snd[:, pc] = total.astype(BF16)
+                chain_copy(j).start()
 
     def inner(g):
         cb = dot(cm[:, g * N : (g + 1) * N], bm[:, g * N : (g + 1) * N], ((1,), (1,)))
@@ -303,21 +354,34 @@
                 parts.append(dot((cb * jnp.exp(gap)).astype(BF16), scaled[p]))
             y[:, pair_cols(p)] += jnp.where(first_head, parts[0], parts[1])
 
-    for k in range(1, chunks):
-        pump(1, k)
-    for g in range(G):
+    for j in range(c_chunks):
+        chain_first(j)
+    inner(0)
+    pump(2, 0)
+    pump(1, 4)
+    for g in range(1, G):
         inner(g)
-    for k in range(max(chunks, c_chunks)):
-        if k < c_chunks:
-            chain(k)
-        if k < chunks:
-            pump(2, k)
     finish(1)
+    chain(0)
+    pump(2, 1)
+
+    def project_z(j, carry):
+        cols = pl.ds(pl.multiple_of(j * tile, tile), tile)
+        acc = dot(xe[pl.ds(HALO, tok), :], wz[:, cols])
+        px[pl.ds(0, tok), cols] = silu(acc.astype(BF16).astype(F32))
+        return carry
+
+    lax.fori_loop(0, width // tile, project_z, 0)
+    for j in range(1, c_chunks - 1):
+        chain(j)
+    pump(2, 2)
+    for j in range(max(1, c_chunks - 1), c_chunks):
+        chain(j)
 
     for g in range(G):
         cols = pl.ds(g * gw, gw)
         reached = dot(cm[:, g * N : (g + 1) * N], car[:, cols])
-        gate = silu(dot(xe[pl.ds(HALO, tok), :], wz[:, cols]).astype(BF16).astype(F32))
+        gate = px[pl.ds(0, tok), cols]
         square = jnp.zeros((tok, 1), F32)
         first = g * per_group // 2
         for p in range(first, first + per_group // 2):
@@ -329,10 +393,17 @@
         inv = lax.rsqrt(square * (1.0 / gw) + EPSILON)
         nrm[:, cols] = (y[:, cols] * inv * scale_ref[:, cols]).astype(BF16)
 
+    pump(2, 3)
+    pump(2, 4)
     finish(2)
     fw = wf.shape[2]
     for d in range(n_dp):
         out_ref[:, d * fw : (d + 1) * fw] = dot(nrm[...], wf[d]).astype(BF16)
+        part = pl.ds(d * fw, fw)
+        pltpu.make_async_copy(out_ref.at[:, part], out_hbm.at[:, part], o_sem.at[d]).start()
+    for d in range(n_dp):
+        part = pl.ds(d * fw, fw)
+        pltpu.make_async_copy(out_ref.at[:, part], out_hbm.at[:, part], o_sem.at[d]).wait()
 
     for copy in sends:
         copy.wait_send()
@@ -363,7 +434,7 @@
     norm_scale_factor,
     final_projection,
 ):
-    n_grp, n_sp, n_dp, chunks, c_chunks = dims
+    n_grp, n_sp, n_dp, c_chunks = dims
     n_x = n_dp // 2
     hidden = mixer_source_array[0]
     tok, model = hidden.shape
@@ -377,8 +448,8 @@
     output = pl.pallas_call(
         functools.partial(kernel, dims),
         out_shape=jax.ShapeDtypeStruct((tok, out_width), BF16),
-        in_specs=[hbm] * 4 + [vmem] * 12,
-        out_specs=vmem,
+        in_specs=[hbm] * 7 + [vmem] * 9,
+        out_specs=hbm,
         scratch_shapes=[
             pltpu.VMEM((HALO + tok, model), BF16),
             pltpu.VMEM((model, width), BF16),
@@ -395,17 +466,23 @@
             pltpu.VMEM((N, width), BF16),
             pltpu.VMEM((N, width), BF16),
             pltpu.VMEM((tok, width), BF16),
-            dma((4,)),
+            pltpu.VMEM((tok, out_width), BF16),
+            pltpu.VMEM((model, 2 * gn), BF16),
+            pltpu.VMEM((increment_projection.shape[1], model), BF16),
+            dma((7,)),
             dma,
             dma,
-            dma((3, remote_srcs, chunks)),
-            dma((3, remote_srcs, chunks)),
-            dma((3, remote_srcs, chunks)),
-            dma((3, remote_srcs)),
-            dma((3, 2 * n_x - 1)),
+            dma((3, remote_srcs, 3)),
+            dma((3, remote_srcs, 3)),
+            dma((3, remote_srcs, 3)),
+            dma((3, remote_srcs, 3)),
+            dma((3, remote_srcs, 2)),
+            dma((3, remote_srcs, 2)),
+            dma((3, n_x, 4)),
             dma((3,)),
             dma((c_chunks,)),
             dma((c_chunks,)),
+            dma((n_dp,)),
         ],
         compiler_params=pltpu.CompilerParams(
             collective_id=0, has_side_effects=True, vmem_limit_bytes=56 * 1024 * 1024
@@ -417,7 +494,7 @@
         final_projection,
         entry_mapping_projection,
         readout_mapping_projection,
-        increment_projection,
+        increment_projection.T,
         source_conv_taps,
         entry_mapping_taps,
         readout_mapping_taps,
@@ -425,7 +502,7 @@
         channel_damping_rate[None],
         bypass_coefficients[None],
         stride_multiplier,
-        added_log_damping,
+        jnp.swapaxes(added_log_damping, 1, 2),
         norm_scale_factor[None],
     )
     return output[None]
@@ -433,9 +510,8 @@
 
 def solution(mesh):
     n_grp, n_sp, n_dp = (mesh.shape[a] for a in ("grp", "sp", "dp"))
-    chunks = 4 if n_dp <= 4 else 1
     return jax.shard_map(
-        functools.partial(shards, (n_grp, n_sp, n_dp, chunks, 4)),
+        functools.partial(shards, (n_grp, n_sp, n_dp, 4)),
         mesh=mesh,
         in_specs=(
             P(("grp", "dp"), "sp", None),

time: 60.1 us -> 51.4 us (0.86)
  Pallas kernels: 55 us -> 49 us
  local copies, waits for them, and re-layouts: 4.84 us -> 2.09 us
    pallas_call x1, Pallas kernels: 55 us -> 49 us  [shards(): pl.pallas_call(functools.partial(kernel, dims), out_shape=jax.ShapeDtypeS...]
    unnamed x5 -> x1, local copies, waits for them, and re-layouts: 4.84 us -> 2.09 us
where the time goes in v2:
time: 51.4 us; the launch traced here: 51.1 us
  Pallas kernels  49 us (95%)
  local copies, waits for them, and re-layouts  2.09 us (4%)
    pallas_call x1, Pallas kernels, shards(): pl.pallas_call(functools.partial(kernel, dims), out_shape=jax.ShapeDtypeS...  49 us
    unnamed x1, local copies, waits for them, and re-layouts  2.09 us

profile of v2, /device:TPU:25, one launch (start us, length us, event | category | flops | bytes accessed | tf_op | source)
XLA Modules:
  0.0 51.1 jit_solution(14614759955272654095)
XLA Ops:
  0.0 49.0 %shard_map.154 = bf16[192,2048]{1,0:T(8,128)(2,1)} custom-call(bf16[192,2048]{1,0:T(8,128)(2,1)} %bitcast.9, bf16[512,1024]{1,0:T(8,128)(2,1)} %wx_hbm.1, bf16[512,1024]{1,0:T(8,128)(2,1)} %wz_hbm.1, bf16[1024,512]{1,0:T(8,128)(2,1)} %wf_hbm.1, bf16[2048,256]{1,0:T(8,128)(2,1)} %wb_hbm.1, bf16[2048,256]{1,0:T(8,128)(2,1)} %wc_hbm.1, ...), custom_call_target="tpu_custom_call" | custom-call | tf_op jit(solution)/shard_map/pallas_call | solution.py:448
  49.1 2.1 %copy.18 = bf16[1,192,2048]{2,1,0:T(8,128)(2,1)} copy(bf16[1,192,2048]{2,1,0:T(8,128)(2,1)} %bitcast.8) | data formatting | bytes 1572864

commit v3 on v2

--- a/solution.py
+++ b/solution.py
@@ -183,7 +183,7 @@
 
     def d_piece(w, o, k, quarter):
         place = at(w, owner_of(o), quarter * 2 * half_of(w), 2 * half_of(w))
-        return remote(place, place, d_send.at[w, o, k], d_recv.at[w], partner)
+        return remote(place, place, d_send.at[w, o, k], d_recv.at[w, 1], partner)
 
     def start(copy):
         copy.start()
@@ -194,7 +194,7 @@
             for o in range(1, n_x):
                 start(x_piece(w, o, k, dp, srcs[w]))
         rows = srcs[w].shape[0]
-        start(remote(srcs[w], at(w, dp, 0, rows), d_send.at[w, 0, 0], d_recv.at[w], partner))
+        start(remote(srcs[w], at(w, dp, 0, rows), d_send.at[w, 0, 0], d_recv.at[w, 0], partner))
 
     def pump(w, k):
         for o in range(1, n_x):
@@ -218,13 +218,22 @@
                 x_piece(w, o, 2, owner_of(o)).wait_recv()
                 start(d_piece(w, o, 3, far_q))
 
-    def finish(w):
+    def finish_near(w):
         own[w].wait()
+        place = at(w, dp, 0, srcs[w].shape[0])
+        remote(place, place, d_send.at[w, 0, 0], d_recv.at[w, 0], partner).wait_recv()
+
+    def finish_far(w):
         if w == 2:
-            place = wf.at[pl.ds(0, n_x)]
+            place = wf.at[pl.ds(0, n_x - 1)]
         else:
-            place = (wx, wz)[w].at[pl.ds(0, n_x * srcs[w].shape[0])]
-        remote(place, place, d_send.at[w, 0, 0], d_recv.at[w], partner).wait_recv()
+            place = (wx, wz)[w].at[pl.ds(0, (n_x - 1) * srcs[w].shape[0])]
+        remote(place, place, d_send.at[w, 1, 0], d_recv.at[w, 1], partner).wait_recv()
+
+    depth = 2 * wx_hbm.shape[0]
+
+    def chip_rows(o):
+        return pl.ds(pl.multiple_of(lax.rem(xi - o + n_x, n_x) * depth, 128), depth)
 
     @pl.when(z == 0)
     def _():
@@ -284,24 +293,48 @@
     def pair_cols(p):
         return pl.ds(p * 2 * P_SIZE, 2 * P_SIZE)
 
-    for k in range(4):
-        pump(0, k)
+    tile = 256
+
+    def tiles(body):
+        def run(j, carry):
+            body(pl.ds(pl.multiple_of(j * tile, tile), tile))
+            return carry
+
+        lax.fori_loop(0, width // tile, run, 0)
+
+    def near_x(cols):
+        px[:, cols] = dot(xe[:, chip_rows(0)], wx[chip_rows(0), cols])
+
+    def far_x(cols):
+        acc = px[:, cols]
+        for o in range(1, n_x):
+            acc = acc + dot(xe[:, chip_rows(o)], wx[chip_rows(o), cols])
+        px[:, cols] = acc.astype(BF16).astype(F32)
+        xs[:, cols] = conv(px, cols, tx_ref[:, cols])
+
+    rows = pl.ds(HALO, tok)
+
+    def near_z(cols):
+        px[pl.ds(0, tok), cols] = dot(xe[rows, chip_rows(0)], wz[chip_rows(0), cols])
+
+    def far_z(cols):
+        acc = px[pl.ds(0, tok), cols]
+        for o in range(1, n_x):
+            acc = acc + dot(xe[rows, chip_rows(o)], wz[chip_rows(o), cols])
+        px[pl.ds(0, tok), cols] = silu(acc.astype(BF16).astype(F32))
+
+    pump(0, 0)
+    pump(0, 1)
+    finish_near(0)
+    tiles(near_x)
+    pump(0, 2)
+    pump(0, 3)
     pump(1, 0)
     pump(0, 4)
-    finish(0)
+    finish_far(0)
     pump(1, 1)
-
-    tile = 256
-
-    def project_x(j, carry):
-        cols = pl.ds(pl.multiple_of(j * tile, tile), tile)
-        px[:, cols] = dot(xe[...], wx[:, cols]).astype(BF16).astype(F32)
-        xs[:, cols] = conv(px, cols, tx_ref[:, cols])
-        return carry
-
-    lax.fori_loop(0, width // tile, project_x, 0)
+    tiles(far_x)
     pump(1, 2)
-    pump(1, 3)
 
     scaled = []
     for p in range(heads // 2):
@@ -354,29 +387,28 @@
                 parts.append(dot((cb * jnp.exp(gap)).astype(BF16), scaled[p]))
             y[:, pair_cols(p)] += jnp.where(first_head, parts[0], parts[1])
 
+    def chain_slot(slot):
+        @pl.when(jnp.minimum(z, 3) == slot)
+        def _():
+            for j in range(c_chunks):
+                chain(j)
+
     for j in range(c_chunks):
         chain_first(j)
+    pump(1, 3)
+    pump(2, 0)
     inner(0)
-    pump(2, 0)
     pump(1, 4)
-    for g in range(1, G):
-        inner(g)
-    finish(1)
-    chain(0)
+    chain_slot(1)
     pump(2, 1)
-
-    def project_z(j, carry):
-        cols = pl.ds(pl.multiple_of(j * tile, tile), tile)
-        acc = dot(xe[pl.ds(HALO, tok), :], wz[:, cols])
-        px[pl.ds(0, tok), cols] = silu(acc.astype(BF16).astype(F32))
-        return carry
-
-    lax.fori_loop(0, width // tile, project_z, 0)
-    for j in range(1, c_chunks - 1):
-        chain(j)
+    inner(1)
     pump(2, 2)
-    for j in range(max(1, c_chunks - 1), c_chunks):
-        chain(j)
+    chain_slot(2)
+    finish_near(1)
+    tiles(near_z)
+    finish_far(1)
+    tiles(far_z)
+    chain_slot(3)
 
     for g in range(G):
         cols = pl.ds(g * gw, gw)
@@ -393,14 +425,23 @@
         inv = lax.rsqrt(square * (1.0 / gw) + EPSILON)
         nrm[:, cols] = (y[:, cols] * inv * scale_ref[:, cols]).astype(BF16)
 
+    fw = wf.shape[2]
+
+    def finish_output(d):
+        part = pl.ds(pl.multiple_of(d * fw, 128), fw)
+        out_ref[:, part] = dot(nrm[...], wf[d]).astype(BF16)
+        pltpu.make_async_copy(out_ref.at[:, part], out_hbm.at[:, part], o_sem.at[d]).start()
+
     pump(2, 3)
+    finish_near(2)
+    finish_output(dp)
+    finish_output(dp + 1 - 2 * core)
     pump(2, 4)
-    finish(2)
-    fw = wf.shape[2]
-    for d in range(n_dp):
-        out_ref[:, d * fw : (d + 1) * fw] = dot(nrm[...], wf[d]).astype(BF16)
-        part = pl.ds(d * fw, fw)
-        pltpu.make_async_copy(out_ref.at[:, part], out_hbm.at[:, part], o_sem.at[d]).start()
+    for o in range(1, n_x):
+        finish_output(owner_of(o))
+    finish_far(2)
+    for o in range(1, n_x):
+        finish_output(owner_of(o) + 1 - 2 * core)
     for d in range(n_dp):
         part = pl.ds(d * fw, fw)
         pltpu.make_async_copy(out_ref.at[:, part], out_hbm.at[:, part], o_sem.at[d]).wait()
@@ -479,7 +520,7 @@
             dma((3, remote_srcs, 2)),
             dma((3, remote_srcs, 2)),
             dma((3, n_x, 4)),
-            dma((3,)),
+            dma((3, 2)),
             dma((c_chunks,)),
             dma((c_chunks,)),
             dma((n_dp,)),

time: 51.4 us -> 46.6 us (0.907)
  Pallas kernels: 49 us -> 44.3 us
    pallas_call x1, Pallas kernels: 49 us -> 44.3 us  [shards(): pl.pallas_call(functools.partial(kernel, dims), out_shape=jax.ShapeDtypeS...]
where the time goes in v3:
time: 46.6 us; the launch traced here: 46.4 us
  Pallas kernels  44.3 us (95%)
  local copies, waits for them, and re-layouts  2.09 us (4%)
    pallas_call x1, Pallas kernels, shards(): pl.pallas_call(functools.partial(kernel, dims), out_shape=jax.ShapeDtypeS...  44.3 us
    unnamed x1, local copies, waits for them, and re-layouts  2.09 us

profile of v3, /device:TPU:25, one launch (start us, length us, event | category | flops | bytes accessed | tf_op | source)
XLA Modules:
  0.0 46.4 jit_solution(11853978585103115347)
XLA Ops:
  0.0 44.3 %shard_map.154 = bf16[192,2048]{1,0:T(8,128)(2,1)} custom-call(bf16[192,2048]{1,0:T(8,128)(2,1)} %bitcast.9, bf16[512,1024]{1,0:T(8,128)(2,1)} %wx_hbm.1, bf16[512,1024]{1,0:T(8,128)(2,1)} %wz_hbm.1, bf16[1024,512]{1,0:T(8,128)(2,1)} %wf_hbm.1, bf16[2048,256]{1,0:T(8,128)(2,1)} %wb_hbm.1, bf16[2048,256]{1,0:T(8,128)(2,1)} %wc_hbm.1, ...), custom_call_target="tpu_custom_call" | custom-call | tf_op jit(solution)/shard_map/pallas_call | solution.py:489
  44.3 2.1 %copy.18 = bf16[1,192,2048]{2,1,0:T(8,128)(2,1)} copy(bf16[1,192,2048]{2,1,0:T(8,128)(2,1)} %bitcast.8) | data formatting | bytes 1572864

commit v4 on v3

--- a/solution.py
+++ b/solution.py
@@ -337,16 +337,6 @@
     pump(1, 2)
 
     scaled = []
-    for p in range(heads // 2):
-        xp = xs[:, pair_cols(p)].astype(F32)
-        s = (xp * spread(step, p, first_head)).astype(BF16)
-        sc[:, pair_cols(p)] = (s.astype(F32) * spread(to_end, p, first_head)).astype(BF16)
-        y[:, pair_cols(p)] = spread(skip_ref[...], p, first_row) * xp
-        scaled.append(s)
-    for g in range(G):
-        cols = pl.ds(g * gw, gw)
-        st[:, cols] = dot(bm[:, g * N : (g + 1) * N], sc[:, cols], ((0,), (0,)))
-
     cw = width // c_chunks
 
     def chain_copy(j):
@@ -385,7 +375,19 @@
             for h in (2 * p, 2 * p + 1):
                 gap = jnp.where(lower, cum[:, h : h + 1] - cum_t[h : h + 1, :], -jnp.inf)
                 parts.append(dot((cb * jnp.exp(gap)).astype(BF16), scaled[p]))
-            y[:, pair_cols(p)] += jnp.where(first_head, parts[0], parts[1])
+            bypass = spread(skip_ref[...], p, first_row) * xs[:, pair_cols(p)].astype(F32)
+            y[:, pair_cols(p)] = jnp.where(first_head, parts[0], parts[1]) + bypass
+
+    def local_state(g):
+        for p in range(g * per_group // 2, (g + 1) * per_group // 2):
+            xp = xs[:, pair_cols(p)].astype(F32)
+            part = (xp * spread(step, p, first_head)).astype(BF16)
+            sc[:, pair_cols(p)] = (part.astype(F32) * spread(to_end, p, first_head)).astype(BF16)
+            scaled.append(part)
+        cols = pl.ds(g * gw, gw)
+        st[:, cols] = dot(bm[:, g * N : (g + 1) * N], sc[:, cols], ((0,), (0,)))
+        for j in range(g * c_chunks // G, (g + 1) * c_chunks // G):
+            chain_first(j)
 
     def chain_slot(slot):
         @pl.when(jnp.minimum(z, 3) == slot)
@@ -393,8 +395,8 @@
             for j in range(c_chunks):
                 chain(j)
 
-    for j in range(c_chunks):
-        chain_first(j)
+    for g in range(G):
+        local_state(g)
     pump(1, 3)
     pump(2, 0)
     inner(0)
@@ -552,7 +554,7 @@
 def solution(mesh):
     n_grp, n_sp, n_dp = (mesh.shape[a] for a in ("grp", "sp", "dp"))
     return jax.shard_map(
-        functools.partial(shards, (n_grp, n_sp, n_dp, 4)),
+        functools.partial(shards, (n_grp, n_sp, n_dp, 8)),
         mesh=mesh,
         in_specs=(
             P(("grp", "dp"), "sp", None),

time: 46.6 us -> 46.3 us (level)
  no operation moved by 1% of the time
where the time goes in v4:
time: 46.3 us; the launch traced here: 46.1 us
  Pallas kernels  44 us (95%)
  local copies, waits for them, and re-layouts  2.09 us (5%)
    pallas_call x1, Pallas kernels, shards(): pl.pallas_call(functools.partial(kernel, dims), out_shape=jax.ShapeDtypeS...  44 us
    unnamed x1, local copies, waits for them, and re-layouts  2.09 us

profile of v4, /device:TPU:25, one launch (start us, length us, event | category | flops | bytes accessed | tf_op | source)
XLA Modules:
  0.0 46.1 jit_solution(9254576028260222316)
XLA Ops:
  0.0 44.0 %shard_map.154 = bf16[192,2048]{1,0:T(8,128)(2,1)} custom-call(bf16[192,2048]{1,0:T(8,128)(2,1)} %bitcast.9, bf16[512,1024]{1,0:T(8,128)(2,1)} %wx_hbm.1, bf16[512,1024]{1,0:T(8,128)(2,1)} %wz_hbm.1, bf16[1024,512]{1,0:T(8,128)(2,1)} %wf_hbm.1, bf16[2048,256]{1,0:T(8,128)(2,1)} %wb_hbm.1, bf16[2048,256]{1,0:T(8,128)(2,1)} %wc_hbm.1, ...), custom_call_target="tpu_custom_call" | custom-call | tf_op jit(solution)/shard_map/pallas_call | solution.py:491
  44.0 2.1 %copy.18 = bf16[1,192,2048]{2,1,0:T(8,128)(2,1)} copy(bf16[1,192,2048]{2,1,0:T(8,128)(2,1)} %bitcast.8) | data formatting | bytes 1572864
